TPU v7x, 256 devices: a whole 4x4x8 slice. The times are simulated.
256 devices in a mesh: sp: 16 (over y, x), dp: 16 (over z, core).
Axes of the slice: x: 4, y: 4, z: 8, core: 2. Of those that a mesh axis runs over, the one named last changes fastest.
Arguments:
- tokens: bfloat16 [16, 6144, 2048], P('dp', 'sp'), may hold values from -6 to 6
- value_act: bfloat16 [16, 6144, 1024], P('dp', 'sp'), may hold values from -6 to 6
- gate_act: bfloat16 [16, 6144, 1024], P('dp', 'sp'), may hold values from -6 to 6
- cotangent: bfloat16 [16, 6144, 1024], P('dp', 'sp'), may hold values from -6 to 6
- value_weight: bfloat16 [2048, 1024], P('dp'), may hold values from -0.1875 to 0.1875
- gate_weight: bfloat16 [2048, 1024], P('dp'), may hold values from -0.1875 to 0.1875
- norm_gain: float32 [1024], replicated, may hold values from 0.1 to 1.9
- norm_bias: float32 [1024], replicated, may hold values from -3 to 3
- mix_weight: bfloat16 [16, 128, 128], replicated, may hold values from -0.5 to 0.5
- mix_bias: float32 [16, 128], replicated, may hold values from 0.1 to 1.9
Outputs:
- tokens_grad: bfloat16 [16, 6144, 2048], P('dp', 'sp')
- value_weight_grad: float32 [2048, 1024], P('dp')
- gate_weight_grad: float32 [2048, 1024], P('dp')
- mix_weight_grad: float32 [16, 128, 128], replicated
- mix_bias_grad: float32 [16, 128], replicated
- norm_gain_grad: float32 [1024], replicated
- norm_bias_grad: float32 [1024], replicated
All inputs are finite; a program needn't handle non-finite values.
Results may differ from a plain program's by a relative error of at most 0.0054.
Values may be sent and summed in bfloat16 or wider, within the bound.
A program may use at most 128 MiB of HBM per device.

v0:
```python
import jax
import jax.numpy as jnp
from jax import lax
from jax.sharding import PartitionSpec as P

EPSILON = 1e-06


def gelu_slope(values):
    cdf_part = 0.5 * (1.0 + lax.erf(values * 0.7071067811865476))
    pdf_part = jnp.exp(-0.5 * values * values) * 0.3989422804014327
    return cdf_part + values * pdf_part


def mixer_backward(value_act, gate_act, cotangent, norm_gain, norm_bias, mix_weight, mix_bias):
    seq_len, channels = value_act.shape
    groups, block_len = (mix_weight.shape[0], mix_weight.shape[1])
    group_dim = channels // groups
    blocks = seq_len // block_len
    value_float = value_act.astype(jnp.float32)
    gate_float = gate_act.astype(jnp.float32)
    activated = jax.nn.gelu(value_float, approximate=False)
    gate_gelu = jax.nn.gelu(gate_float, approximate=False)
    centred = gate_gelu - jnp.mean(gate_gelu, axis=-1, keepdims=True)
    inv_std = lax.rsqrt(jnp.mean(centred * centred, axis=-1, keepdims=True) + EPSILON)
    normed = centred * inv_std
    spread_in = (normed * norm_gain + norm_bias).astype(jnp.bfloat16)
    spread_in = spread_in.reshape(blocks, block_len, groups, group_dim)
    causal = jnp.tril(jnp.ones((block_len, block_len), dtype=bool))
    masked_weight = jnp.where(causal[None], mix_weight, jnp.zeros_like(mix_weight))
    spatial = jnp.einsum(
        "gts,bsgd->btgd", masked_weight, spread_in, preferred_element_type=jnp.float32
    )
    spatial = (spatial + mix_bias.T[None, :, :, None]).reshape(seq_len, channels)
    grad_out = cotangent.astype(jnp.float32)
    grad_act = grad_out * spatial
    grad_spatial = grad_out * activated
    grad_split = grad_spatial.reshape(blocks, block_len, groups, group_dim)
    bias_grad = jnp.sum(grad_split, axis=(0, 3)).T
    spatial_low = grad_split.astype(jnp.bfloat16)
    weight_grad = jnp.einsum(
        "btgd,bsgd->gts", spatial_low, spread_in, preferred_element_type=jnp.float32
    )
    weight_grad = jnp.where(causal[None], weight_grad, jnp.zeros_like(weight_grad))
    grad_norm = jnp.einsum(
        "gts,btgd->bsgd", masked_weight, spatial_low, preferred_element_type=jnp.float32
    )
    grad_norm = grad_norm.reshape(seq_len, channels)
    gain_grad = jnp.sum(grad_norm * normed, axis=0)
    shift_grad = jnp.sum(grad_norm, axis=0)
    grad_hat = grad_norm * norm_gain
    grad_gate = inv_std * (
        grad_hat
        - jnp.mean(grad_hat, axis=-1, keepdims=True)
        - normed * jnp.mean(grad_hat * normed, axis=-1, keepdims=True)
    )
    value_grad = (grad_act * gelu_slope(value_float)).astype(jnp.bfloat16)
    gate_grad = (grad_gate * gelu_slope(gate_float)).astype(jnp.bfloat16)
    return (value_grad, gate_grad, (weight_grad, bias_grad, gain_grad, shift_grad))


def shards(
    tokens,
    value_act,
    gate_act,
    cotangent,
    value_weight,
    gate_weight,
    norm_gain,
    norm_bias,
    mix_weight,
    mix_bias,
):
    value_grad, gate_grad, stats = mixer_backward(
        value_act[0], gate_act[0], cotangent[0], norm_gain, norm_bias, mix_weight, mix_bias
    )
    channels = value_grad.shape[1]
    both_grads = jnp.concatenate((value_grad, gate_grad), axis=1)
    both_weights = jnp.concatenate((value_weight, gate_weight), axis=1)
    input_grad = lax.dot_general(
        both_grads,
        lax.all_gather(both_weights, "dp", axis=0, tiled=True),
        (((1,), (1,)), ((), ())),
        preferred_element_type=jnp.float32,
    ).astype(jnp.bfloat16)
    inputs = tokens[0]
    shard_terms = lax.psum_scatter(
        lax.dot_general(
            inputs, both_grads, (((0,), (0,)), ((), ())), preferred_element_type=jnp.float32
        ),
        "dp",
        scatter_dimension=0,
        tiled=True,
    )
    weight_sums = lax.psum(shard_terms, "sp")
    totals = lax.psum((stats[0], stats[1], stats[2], stats[3]), ("sp", "dp"))
    return (
        input_grad[None],
        weight_sums[:, :channels],
        weight_sums[:, channels:],
        totals[0],
        totals[1],
        totals[2],
        totals[3],
    )


def solution(mesh):
    placed = (
        P("dp", "sp", None),
        P("dp", "sp", None),
        P("dp", "sp", None),
        P("dp", "sp", None),
        P("dp", None),
        P("dp", None),
        P(),
        P(),
        P(),
        P(),
    )
    return jax.shard_map(
        shards,
        mesh=mesh,
        in_specs=placed,
        out_specs=(P("dp", "sp", None), P("dp", None), P("dp", None), P(), P(), P(), P()),
        check_vma=False,
    )
```

profile of v0, /device:TPU:2, one launch (start us, length us, event | category | flops | bytes accessed | tf_op | source)
XLA Modules:
  0.0 603.1 jit_solution(7592910926025882119)
XLA Ops:
  7.2 2.4 copy.20
  9.6 4.5 fusion.96
  14.2 1.9 convert_multiply_fusion.1
  16.2 2.3 copy.28
  18.5 2.3 copy.19
  21.1 3.4 reshape.153
  24.6 3.0 convert_multiply_fusion
  27.6 3.6 mul.200
  31.1 3.6 mul.202
  34.7 3.6 mul.177
  38.3 3.6 mul.179
  41.9 5.6 fusion.93
  47.6 4.0 multiply_reduce_fusion
  56.9 1.5 fusion.79
  59.4 9.4 %convolution_bitcast_fusion = f32[2048,2048]{0,1:T(8,128)} fusion(bf16[1,384,2048]{2,1,0:T(8,128)(2,1)S(1)} %copy-done, bf16[384,1024]{0,1:T(8,128)(2,1)S(1)} %fusion.79, bf16[384,1024]{0,1:T(8,128)(2,1)S(1)} %fusion.78), kind=kOutput, calls=%fused_computation | convolution fusion | flops 3224371200 | bytes 19922944 | tf_op jit(solution)/shard_map/dot_general | solution.py:88
  69.7 1.8 pad_maximum_fusion.3
  71.5 100.9 %reduce-scatter.2.cloned.1.call-done = f32[128,2048]{0,1:T(8,128)} async-done(((f32[2048,2048]{0,1:T(8,128)}), f32[128,2048]{0,1:T(8,128)}) %reduce-scatter.2.cloned.1.call-update) | async-done | bytes 1048592 | tf_op jit(solution)/shard_map/reduce_scatter | solution.py:87
  172.7 2.9 fusion.80
  175.8 77.8 %all-reduce = (f32[16,128]{1,0:T(8,128)}, f32[1024]{0:T(1024)}, f32[1024]{0:T(1024)}) all-reduce(f32[16,128]{1,0:T(8,128)S(1)} %bitcast.235, f32[1024]{0:T(1024)S(1)} %reduce_sum.73, f32[1024]{0:T(1024)S(1)} %reduce_sum.75), channel_id=1, replica_groups=mesh['sp'=16,'dp'=16] {'sp','dp'}, use_global_device_ids=true, to_apply=%region_8.9 | all-reduce | flops 4096 | bytes 32768 | tf_op jit(solution)/shard_map/psum | solution.py:96
  253.6 8.6 %fusion = bf16[1,384,2048]{2,1,0:T(8,128)(2,1)} fusion(bf16[2048,2048]{1,0:T(8,128)(2,1)} %all-gather.2.cloned.1.call-done, bf16[384,1024]{0,1:T(8,128)(2,1)} %copy-done.8, bf16[384,1024]{0,1:T(8,128)(2,1)} %copy-done.7), kind=kOutput, calls=%fused_computation.2 | convolution fusion | flops 3225157632 | bytes 11534336 | tf_op jit(solution)/shard_map/dot_general | solution.py:80
  262.2 67.5 %all-reduce.4.cloned.1.call-done = f32[128,2048]{0,1:T(8,128)} async-done(((f32[128,2048]{0,1:T(8,128)}), f32[128,2048]{0,1:T(8,128)}) %all-reduce.4.cloned.1.call-update) | async-done | bytes 1048592 | tf_op jit(solution)/shard_map/psum | solution.py:95
  329.6 1.3 fusion.98
  332.9 261.4 %all-reduce.6.cloned.1.call-done = f32[16,128,128]{2,1,0:T(8,128)} async-done(((f32[16,128,128]{2,1,0:T(8,128)}), f32[16,128,128]{2,1,0:T(8,128)}) %all-reduce.6.cloned.1.call-update) | async-done | bytes 1048592 | tf_op jit(solution)/shard_map/psum | solution.py:96
  594.3 2.3 copy.61
  (58 shorter events, 10.0 us)
Async XLA Ops:
  7.2 52.2 %copy-start = (bf16[1,384,2048]{2,1,0:T(8,128)(2,1)S(1)}, bf16[1,384,2048]{2,1,0:T(8,128)(2,1)}, u32[]{:S(2)}) copy-start(bf16[1,384,2048]{2,1,0:T(8,128)(2,1)} %param.10) | copy-start | bytes 4718596
  7.2 165.2 %reduce-scatter.2.cloned.1.call-start = ((), (), s32[]{:S(2)}) async-start(), calls=%async_computation.2 | async-start | bytes 17825792 | tf_op jit(solution)/shard_map/reduce_scatter | solution.py:87
  9.6 4.5 copy-start.1
  14.2 1.9 copy-start.14
  14.2 2.0 copy-start.16
  41.9 5.6 copy-start.10
  41.9 5.6 copy-start.11
  41.9 5.7 copy-start.12
  47.6 4.1 copy-start.9
  47.6 5.2 copy-start.15
  51.6 1.1 copy-start.5
  53.3 1.1 copy-start.3
  53.3 1.4 copy-start.4
  55.5 2.9 copy-start.7
  55.5 1.4 copy-start.2
  58.4 0.9 copy-start.8
  68.7 0.9 copy-start.13
  68.8 103.9 %copy-start.6 = (f32[3,128,16,64]{1,3,0,2:T(8,128)S(1)}, f32[3,128,16,64]{1,3,0,2:T(8,128)}, u32[]{:S(2)}) copy-start(f32[3,128,16,64]{1,3,0,2:T(8,128)} %copy-done.5) | copy-start | bytes 4718596
  68.8 184.8 %all-gather.2.cloned.1.call-start = ((), (), s32[]{:S(2)}) async-start(), calls=%async_computation.1 | async-start | bytes 8912896 | tf_op jit(solution)/shard_map/all_gather | solution.py:82
  71.5 258.2 %all-reduce.4.cloned.1.call-start = ((), (), s32[]{:S(2)}) async-start(), calls=%async_computation.3 | async-start | bytes 2097152 | tf_op jit(solution)/shard_map/psum | solution.py:95
  172.4 421.8 %all-reduce.6.cloned.1.call-start = ((), (), s32[]{:S(2)}) async-start(), calls=%async_computation.4 | async-start | bytes 2097152 | tf_op jit(solution)/shard_map/psum | solution.py:96
Sparse Core Ops, SparseCore 0:
  68.9 103.4 reduce-scatter.1
  174.8 55.9 all-gather.1
  234.0 95.5 all-reduce.3
  335.5 258.7 all-reduce.5
where the time goes:
time: 604 us; the launch traced here: 603 us
  waiting for transfers between devices  430 us (71%)
  blocking collectives  77.8 us (13%)
  local copies, waits for them, and re-layouts  36.4 us (6%)
  matrix products  25.4 us (4%)
  other arithmetic  19.3 us (3%)
  between operations  14 us (2%)
    psum x1, waiting for transfers between devices, shards(): totals = lax.psum((stats[0], stats[1], stats[2], stats[3]), ('sp', 'dp'))  261 us
    reduce_scatter x1, waiting for transfers between devices, shards(): lax.psum_scatter(lax.dot_general(inputs, both_grads, (((0,), (0,)), ((),...  101 us
    psum x1, blocking collectives, shards(): totals = lax.psum((stats[0], stats[1], stats[2], stats[3]), ('sp', 'dp'))  77.8 us
    psum x1, waiting for transfers between devices, shards(): weight_sums = lax.psum(shard_terms, 'sp')  67.5 us
    unnamed x40, local copies, waits for them, and re-layouts  14.9 us
  transfers between devices with their start and end apart: 4, of which 3 were waited for; matrix products, arithmetic and copies ran while one was open for 3% of the time, Pallas kernels for 0%

commit v1 on v0

--- a/solution.py
+++ b/solution.py
@@ -92,7 +92,16 @@
         scatter_dimension=0,
         tiled=True,
     )
-    weight_sums = lax.psum(shard_terms, "sp")
+    weight_sums = shard_terms
+    axis_len = lax.axis_size("sp")
+    for dev in [pp for pp in (1, 2, 4, 8, 16) if pp < axis_len]:
+        queue = []
+        b = 0
+        while b < axis_len:
+            queue.append((b, b ^ dev))
+            b += 1
+        piece_now = lax.ppermute(weight_sums, axis_name="sp", perm=queue)
+        weight_sums = weight_sums + piece_now
     totals = lax.psum((stats[0], stats[1], stats[2], stats[3]), ("sp", "dp"))
     return (
         input_grad[None],

time: 604 us -> 498 us (0.82)
  waiting for transfers between devices: 430 us -> 304 us
  blocking collectives: 77.8 us -> 89.4 us
  starting transfers between devices: 0.38 us -> 6.8 us
    psum x1, waiting for transfers between devices: 261 us -> 141 us  [shards(): totals = lax.psum((stats[0], stats[1], stats[2], stats[3]), ('sp', 'dp'))]
    psum x1 -> x0, waiting for transfers between devices: 67.5 us -> none  [shards(): weight_sums = lax.psum(shard_terms, 'sp')]
    ppermute x0 -> x4, waiting for transfers between devices: none -> 61.6 us  [shards(): piece_now = lax.ppermute(weight_sums, axis_name='sp', perm=queue)]
    psum x1, blocking collectives: 77.8 us -> 89.4 us  [shards(): totals = lax.psum((stats[0], stats[1], stats[2], stats[3]), ('sp', 'dp'))]
    ppermute x0 -> x4, starting transfers between devices: none -> 6.68 us  [shards(): piece_now = lax.ppermute(weight_sums, axis_name='sp', perm=queue)]
    unnamed x40 -> x48, local copies, waits for them, and re-layouts: 14.9 us -> 15 us
  transfers between devices with their start and end apart: 4 -> 7, of which waited for: 3 -> 5; matrix products, arithmetic and copies ran while one was open for 3% -> 3% of each run, Pallas kernels for 0% -> 0%
where the time goes in v1:
time: 498 us; the launch traced here: 497 us
  waiting for transfers between devices  304 us (61%)
  blocking collectives  89.4 us (18%)
  local copies, waits for them, and re-layouts  35.3 us (7%)
  matrix products  24 us (5%)
  other arithmetic  21.4 us (4%)
  between operations  15.7 us (3%)
  starting transfers between devices  6.8 us (1%)
    psum x1, waiting for transfers between devices, shards(): totals = lax.psum((stats[0], stats[1], stats[2], stats[3]), ('sp', 'dp'))  141 us
    reduce_scatter x1, waiting for transfers between devices, shards(): lax.psum_scatter(lax.dot_general(inputs, both_grads, (((0,), (0,)), ((),...  102 us
    psum x1, blocking collectives, shards(): totals = lax.psum((stats[0], stats[1], stats[2], stats[3]), ('sp', 'dp'))  89.4 us
    ppermute x4, waiting for transfers between devices, shards(): piece_now = lax.ppermute(weight_sums, axis_name='sp', perm=queue)  61.6 us
    unnamed x48, local copies, waits for them, and re-layouts  15 us
  transfers between devices with their start and end apart: 7, of which 5 were waited for; matrix products, arithmetic and copies ran while one was open for 3% of the time, Pallas kernels for 0%

profile of v1, /device:TPU:2, one launch (start us, length us, event | category | flops | bytes accessed | tf_op | source)
XLA Modules:
  0.0 497.2 jit_solution(16014844902752506183)
XLA Ops:
  8.1 2.4 copy.20
  10.5 4.5 fusion.96
  15.0 1.9 convert_multiply_fusion.1
  17.1 2.3 copy.28
  19.4 2.4 copy.19
  22.0 3.4 reshape.153
  25.4 3.0 convert_multiply_fusion
  28.4 3.6 mul.200
  32.0 3.6 mul.202
  35.6 3.6 mul.177
  39.2 3.6 mul.179
  42.8 5.6 %fusion.93 = (f32[128,16]{0,1:T(8,128)S(1)}, bf16[3,128,16,64]{1,3,0,2:T(8,128)(2,1)S(1)}) fusion(f32[3,128,16,64]{1,0,3,2:T(4,128)} %mul.202, f32[3,128,16,64]{1,0,3,2:T(4,128)} %mul.200, f32[3,128,16,64]{1,0,3,2:T(4,128)} %reshape.153), kind=kLoop, calls=%fused_computation.137 | loop fusion | flops 25163776 | bytes 5513216 | tf_op jit(solution)/shard_map/reduce_sum | solution.py:39
  48.5 4.0 multiply_reduce_fusion
  60.2 9.4 %convolution_bitcast_fusion = f32[2048,2048]{0,1:T(8,128)} fusion(bf16[1,384,2048]{2,1,0:T(8,128)(2,1)S(1)} %copy-done, bf16[384,1024]{0,1:T(8,128)(2,1)S(1)} %fusion.79, bf16[384,1024]{0,1:T(8,128)(2,1)S(1)} %fusion.78), kind=kOutput, calls=%fused_computation | convolution fusion | flops 3224371200 | bytes 19922944 | tf_op jit(solution)/shard_map/dot_general | solution.py:88
  71.6 101.7 %reduce-scatter.2.cloned.1.call-done = f32[128,2048]{0,1:T(8,128)} async-done(((f32[2048,2048]{0,1:T(8,128)}), f32[128,2048]{0,1:T(8,128)}) %reduce-scatter.2.cloned.1.call-update) | async-done | bytes 1048592 | tf_op jit(solution)/shard_map/reduce_scatter | solution.py:87
  173.8 23.5 %collective-permute-done = f32[128,2048]{0,1:T(8,128)S(1)} collective-permute-done((f32[128,2048]{0,1:T(8,128)}, f32[128,2048]{0,1:T(8,128)S(1)}, u32[]{:S(2)}, u32[]{:S(2)}) %collective-permute-start) | collective-permute-done | bytes 1048608 | tf_op jit(solution)/shard_map/ppermute | solution.py:103
  198.7 2.4 collective-permute-start.1
  201.1 22.5 %collective-permute-done.1 = f32[128,2048]{0,1:T(8,128)S(1)} collective-permute-done((f32[128,2048]{0,1:T(8,128)S(1)}, f32[128,2048]{0,1:T(8,128)S(1)}, u32[]{:S(2)}, u32[]{:S(2)}) %collective-permute-start.1) | collective-permute-done | bytes 1048608 | tf_op jit(solution)/shard_map/ppermute | solution.py:103
  227.3 89.4 %all-reduce = (f32[16,128]{1,0:T(8,128)}, f32[1024]{0:T(1024)}, f32[1024]{0:T(1024)}) all-reduce(f32[16,128]{1,0:T(8,128)S(1)} %bitcast.235, f32[1024]{0:T(1024)S(1)} %reduce_sum.73, f32[1024]{0:T(1024)S(1)} %reduce_sum.75), channel_id=1, replica_groups=mesh['sp'=16,'dp'=16] {'sp','dp'}, use_global_device_ids=true, to_apply=%region_7.8 | all-reduce | flops 4096 | bytes 32768 | tf_op jit(solution)/shard_map/psum | solution.py:105
  318.1 2.2 collective-permute-start.3
  320.3 8.3 %fusion = bf16[1,384,2048]{2,1,0:T(8,128)(2,1)} fusion(bf16[2048,2048]{1,0:T(8,128)(2,1)} %all-gather.2.cloned.1.call-done, bf16[384,1024]{0,1:T(8,128)(2,1)} %copy-done.10, bf16[384,1024]{0,1:T(8,128)(2,1)S(1)} %copy-done.9), kind=kOutput, calls=%fused_computation.2 | convolution fusion | flops 3225157632 | bytes 11534336 | tf_op jit(solution)/shard_map/dot_general | solution.py:80
  328.6 15.6 %collective-permute-done.3 = f32[128,2048]{0,1:T(8,128)S(1)} collective-permute-done((f32[128,2048]{0,1:T(8,128)S(1)}, f32[128,2048]{0,1:T(8,128)S(1)}, u32[]{:S(2)}, u32[]{:S(2)}) %collective-permute-start.3) | collective-permute-done | bytes 1048608 | tf_op jit(solution)/shard_map/ppermute | solution.py:103
  346.4 141.1 %all-reduce.3.cloned.1.call-done = f32[16,128,128]{2,1,0:T(8,128)} async-done(((f32[16,128,128]{2,1,0:T(8,128)}), f32[16,128,128]{2,1,0:T(8,128)}) %all-reduce.3.cloned.1.call-update) | async-done | bytes 1048592 | tf_op jit(solution)/shard_map/psum | solution.py:105
  487.5 2.3 copy.60
  (75 shorter events, 19.1 us)
Async XLA Ops:
  8.0 52.2 %copy-start = (bf16[1,384,2048]{2,1,0:T(8,128)(2,1)S(1)}, bf16[1,384,2048]{2,1,0:T(8,128)(2,1)}, u32[]{:S(2)}) copy-start(bf16[1,384,2048]{2,1,0:T(8,128)(2,1)} %param.10) | copy-start | bytes 4718596
  8.0 165.3 %reduce-scatter.2.cloned.1.call-start = ((), (), s32[]{:S(2)}) async-start(), calls=%async_computation.2 | async-start | bytes 17825792 | tf_op jit(solution)/shard_map/reduce_scatter | solution.py:87
  10.5 4.5 copy-start.2
  15.0 1.9 copy-start.18
  15.0 2.0 copy-start.20
  42.8 5.6 %copy-start.13 = (f32[3,128,16,64]{1,0,3,2:T(4,128)S(1)}, f32[3,128,16,64]{1,0,3,2:T(4,128)}, u32[]{:S(2)}) copy-start(f32[3,128,16,64]{1,0,3,2:T(4,128)} %mul.177) | copy-start | bytes 4718596
  42.8 5.6 %copy-start.14 = (f32[3,128,16,64]{1,0,3,2:T(4,128)S(1)}, f32[3,128,16,64]{1,0,3,2:T(4,128)}, u32[]{:S(2)}) copy-start(f32[3,128,16,64]{1,0,3,2:T(4,128)} %mul.179) | copy-start | bytes 4718596
  42.8 5.7 %copy-start.15 = (bf16[16,128,128]{2,1,0:T(8,128)(2,1)S(1)}, bf16[16,128,128]{2,1,0:T(8,128)(2,1)}, u32[]{:S(2)}) copy-start(bf16[16,128,128]{2,1,0:T(8,128)(2,1)} %param.18) | copy-start | bytes 1572868
  48.5 4.1 copy-start.11
  48.5 5.2 %copy-start.19 = (f32[16,128]{1,0:T(8,128)S(1)}, f32[16,128]{1,0:T(8,128)}, u32[]{:S(2)}) copy-start(f32[16,128]{1,0:T(8,128)} %param.19) | copy-start | bytes 24580
  52.6 1.1 copy-start.6
  54.3 1.4 copy-start.5
  56.4 2.9 copy-start.8
  56.4 1.4 copy-start.3
  69.6 250.7 %all-gather.2.cloned.1.call-start = ((), (), s32[]{:S(2)}) async-start(), calls=%async_computation.1 | async-start | bytes 8912896 | tf_op jit(solution)/shard_map/all_gather | solution.py:82
  71.5 416.0 %all-reduce.3.cloned.1.call-start = ((), (), s32[]{:S(2)}) async-start(), calls=%async_computation.3 | async-start | bytes 2097152 | tf_op jit(solution)/shard_map/psum | solution.py:105
  173.3 24.0 %collective-permute-start = (f32[128,2048]{0,1:T(8,128)}, f32[128,2048]{0,1:T(8,128)S(1)}, u32[]{:S(2)}, u32[]{:S(2)}) collective-permute-start(f32[128,2048]{0,1:T(8,128)} %reduce-scatter.2.cloned.1.call-done), channel_id=1, source_target_pairs={{0,16},{16,0},{32,48},{48,32},{64,80},{80,64},{96,112},{112,96},{1... | collective-permute-start | bytes 3145736 | tf_op jit(solution)/shard_map/ppermute | solution.py:103
  198.7 26.6 %copy-start.7 = (f32[3,128,16,64]{1,3,0,2:T(8,128)S(1)}, f32[3,128,16,64]{1,3,0,2:T(8,128)}, u32[]{:S(2)}) copy-start(f32[3,128,16,64]{1,3,0,2:T(8,128)} %copy-done.6) | copy-start | bytes 4718596
  198.7 26.6 %copy-start.12 = (bf16[3,128,16,64]{1,3,0,2:T(8,128)(2,1)S(1)}, bf16[3,128,16,64]{1,3,0,2:T(8,128)(2,1)}, u32[]{:S(2)}) copy-start(bf16[3,128,16,64]{1,3,0,2:T(8,128)(2,1)} %copy-done.11) | copy-start | bytes 2359300
  198.7 24.9 %collective-permute-start.1 = (f32[128,2048]{0,1:T(8,128)S(1)}, f32[128,2048]{0,1:T(8,128)S(1)}, u32[]{:S(2)}, u32[]{:S(2)}) collective-permute-start(f32[128,2048]{0,1:T(8,128)S(1)} %add.77), channel_id=1, source_target_pairs={{0,32},{16,48},{32,0},{48,16},{64,96},{80,112},{96,64},{112,80},{1... | collective-permute-start | bytes 3145736 | tf_op jit(solution)/shard_map/ppermute | solution.py:103
  223.7 93.0 %collective-permute-start.2 = (f32[128,2048]{0,1:T(8,128)S(1)}, f32[128,2048]{0,1:T(8,128)}, u32[]{:S(2)}, u32[]{:S(2)}) collective-permute-start(f32[128,2048]{0,1:T(8,128)S(1)} %add.78), channel_id=1, source_target_pairs={{0,64},{16,80},{32,96},{48,112},{64,0},{80,16},{96,32},{112,48},{1... | collective-permute-start | bytes 3145736 | tf_op jit(solution)/shard_map/ppermute | solution.py:103
  316.7 3.6 copy-start.9
  318.1 26.1 %collective-permute-start.3 = (f32[128,2048]{0,1:T(8,128)S(1)}, f32[128,2048]{0,1:T(8,128)S(1)}, u32[]{:S(2)}, u32[]{:S(2)}) collective-permute-start(f32[128,2048]{0,1:T(8,128)S(1)} %add.79), channel_id=1, source_target_pairs={{0,128},{16,144},{32,160},{48,176},{64,192},{80,208},{96,224},{112... | collective-permute-start | bytes 3145736 | tf_op jit(solution)/shard_map/ppermute | solution.py:103
  345.4 144.4 %copy-start.1 = (bf16[1,384,2048]{2,1,0:T(8,128)(2,1)S(1)}, bf16[1,384,2048]{2,1,0:T(8,128)(2,1)}, u32[]{:S(2)}) copy-start(bf16[1,384,2048]{2,1,0:T(8,128)(2,1)} %param.10) | copy-start | bytes 4718596
  (4 other events, 4.0 us)
Sparse Core Ops, SparseCore 0:
  69.8 103.4 reduce-scatter.1
  175.7 54.7 all-gather.1
Sparse Core Ops, SparseCore 1:
  227.2 260.2 all-reduce.2
